TPU v7x, 512 devices: a whole 4x8x8 slice. The times are simulated.
512 devices in a mesh: row: 32 (over z, x), col: 16 (over y, core).
Axes of the slice: x: 4, y: 8, z: 8, core: 2. Of those that a mesh axis runs over, the one named last changes fastest.
Arguments:
- tokens: bfloat16 [32768, 2048], P('row'), may hold values from -136 to 136
- norm_gain: float32 [2048], replicated, may hold values from 0.1 to 1.9
- w_in: bfloat16 [2048, 1024], P(None, 'col'), may hold values from -0.125 to 0.125
- w_out: bfloat16 [1024, 2048], P(None, 'col'), may hold values from -0.1875 to 0.1875
Outputs:
- mixed_tokens: bfloat16 [32768, 2048], P('row', 'col')
All inputs are finite; a program needn't handle non-finite values.
Results may differ from a plain program's by a relative error of at most 0.013.
Values may be sent and summed in bfloat16 or wider, within the bound.
No kernel may reach another device: no remote copies, remote signals or barrier semaphores. Data moves between devices by JAX's collectives and lax.ppermute only.
A program may use at most 64 MiB of HBM per device.

v0:
```python
import math
import jax
import jax.numpy as jnp
from jax import lax
from jax.sharding import PartitionSpec as P

GROUP = 256
NORM_EPS = 1e-06


def in_one_piece(arrays, axis, split_dim, concat_dim, along):
    ends, at = ([], 0)
    for a in arrays[:-1]:
        at += a.shape[along]
        ends.append(at)
    both = jnp.concatenate(arrays, axis=along)
    return tuple(
        jnp.split(
            lax.all_to_all(both, axis, split_axis=split_dim, concat_axis=concat_dim, tiled=True),
            ends,
            axis=along,
        )
    )


def as_sent(array):

    def short(part):
        return part.astype(jnp.bfloat16) if part.dtype == jnp.float32 else part

    return jax.tree.map(short, array)


def rotation_table(first_index, second_index, spectral_magnitude, factor):
    phase = (first_index * second_index % spectral_magnitude).astype(jnp.float32) * (
        2.0 * math.pi / spectral_magnitude
    )
    return (jnp.cos(phase) * factor, jnp.sin(phase) * factor)


def twiddle(real_input_values, imag_in, freq_index, pos_index, spectral_magnitude):
    cosine, sine = rotation_table(freq_index, pos_index, spectral_magnitude, 1.0)
    return (
        real_input_values * cosine + imag_in * sine,
        imag_in * cosine - real_input_values * sine,
    )


def second_section(stacked, half):
    length_dev = stacked.shape[1]
    stride = min(length_dev, 512)
    positions = lax.broadcasted_iota(jnp.int32, (length_dev, stride), 0)
    real_blocks = []
    imag_blocks = []
    for offset in range(0, length_dev, stride):
        freqs = lax.broadcasted_iota(jnp.int32, (length_dev, stride), 1) + offset
        cosine, sine = rotation_table(positions, freqs, length_dev, 1.0)
        with_cos = jnp.dot(stacked, cosine, precision=lax.Precision.HIGH)
        with_sin = jnp.dot(stacked, sine, precision=lax.Precision.HIGH)
        real_blocks.append(with_cos[:half] + with_sin[half:])
        imag_blocks.append(with_cos[half:] - with_sin[:half])
    return (jnp.concatenate(real_blocks, 1), jnp.concatenate(imag_blocks, 1))


def reorder_positions(arrived):
    channels, row_count, _, block_len = arrived.shape
    return jnp.swapaxes(arrived.reshape(channels, row_count, block_len), 1, 2).reshape(
        channels, row_count * block_len
    )


def local(tokens, norm_gain, w_in, w_out):
    length_dev = tokens.shape[0]
    row_count = lax.axis_size("row")
    col_count = lax.axis_size("col")
    total_len = length_dev * row_count
    widened = tokens.astype(jnp.float32)
    inverse = lax.rsqrt(jnp.mean(widened * widened, axis=1, keepdims=True) + NORM_EPS)
    normed = (widened * inverse * norm_gain[None, :]).astype(jnp.bfloat16)
    projected = lax.dot_general(
        w_in, normed, (((0,), (1,)), ((), ())), preferred_element_type=jnp.float32
    ).astype(jnp.bfloat16)
    channels = projected.shape[0]
    block_len = length_dev // row_count
    small_cos, small_sin = rotation_table(
        lax.broadcasted_iota(jnp.int32, (row_count, row_count), 0),
        lax.broadcasted_iota(jnp.int32, (row_count, row_count), 1),
        row_count,
        1.0 / math.sqrt(total_len),
    )
    per_row = channels // row_count
    arrived = lax.all_to_all(
        projected.reshape(channels, 1, length_dev), "row", split_axis=0, concat_axis=1, tiled=True
    )
    values = arrived.astype(jnp.float32)
    real_one = jnp.einsum("ka,cab->ckb", small_cos, values, precision=lax.Precision.HIGH)
    imag_one = -jnp.einsum("ka,cab->ckb", small_sin, values, precision=lax.Precision.HIGH)
    freq_index = lax.broadcasted_iota(jnp.int32, (row_count, length_dev), 0)
    pos_index = lax.broadcasted_iota(jnp.int32, (row_count, length_dev), 1)
    real_two, imag_two = twiddle(real_one, imag_one, freq_index, pos_index, total_len)
    stacked = jnp.concatenate(
        [
            real_two.reshape(per_row * row_count, length_dev),
            imag_two.reshape(per_row * row_count, length_dev),
        ],
        0,
    )
    real_three, imag_three = second_section(stacked, per_row * row_count)
    shaped = (per_row, row_count, row_count, block_len)
    back_real, back_imag = tuple(
        (
            part.astype(jnp.float32)
            for part in in_one_piece(
                (
                    real_three.reshape(shaped).astype(jnp.bfloat16),
                    imag_three.reshape(shaped).astype(jnp.bfloat16),
                ),
                "row",
                2,
                0,
                1,
            )
        )
    )
    spec_real = reorder_positions(back_real)
    spec_imag = reorder_positions(back_imag)
    quarter = length_dev // col_count
    group_cosine_table, group_sine_table = rotation_table(
        lax.broadcasted_iota(jnp.int32, (GROUP, GROUP), 0),
        lax.broadcasted_iota(jnp.int32, (GROUP, GROUP), 1),
        GROUP,
        1.0 / math.sqrt(GROUP),
    )
    real_input_values = lax.all_to_all(
        as_sent(spec_real.reshape(channels, col_count, quarter)),
        "col",
        split_axis=1,
        concat_axis=0,
        tiled=True,
    )
    imag_in = lax.all_to_all(
        as_sent(spec_imag.reshape(channels, col_count, quarter)),
        "col",
        split_axis=1,
        concat_axis=0,
        tiled=True,
    )
    width_all = real_input_values.shape[0]
    item_count = real_input_values.shape[2]
    groups = width_all // GROUP
    real_by_group = real_input_values.reshape(groups, GROUP, item_count)
    imaginary_by_group = imag_in.reshape(groups, GROUP, item_count)
    merged_spectrum = jnp.einsum(
        "hz,azo->aho", group_cosine_table, real_by_group, precision=lax.Precision.HIGH
    )
    merged_spectrum = merged_spectrum + jnp.einsum(
        "hz,azo->aho", group_sine_table, imaginary_by_group, precision=lax.Precision.HIGH
    )
    result = merged_spectrum.reshape(width_all, 1, item_count).astype(jnp.bfloat16)
    portion = lax.all_gather(result, "col", axis=2, tiled=True)
    flat = portion.reshape(portion.shape[0], portion.shape[2])
    output = lax.dot_general(
        flat, w_out, (((0,), (0,)), ((), ())), preferred_element_type=jnp.float32
    )
    return output.astype(jnp.bfloat16)


def solution(mesh):
    placed = (P("row", None), P(), P(None, "col"), P(None, "col"))
    return jax.shard_map(
        local, mesh=mesh, in_specs=placed, out_specs=P("row", "col"), check_vma=False
    )
```

profile of v0, /device:TPU:1, one launch (start us, length us, event | category | flops | bytes accessed | tf_op | source)
XLA Modules:
  0.0 170.5 jit_solution(13047247857492114618)
XLA Ops:
  6.5 3.2 %fusion = f32[1024]{0:T(1024)S(1)} fusion(bf16[1024,2048]{1,0:T(8,128)(2,1)} %param.4), kind=kLoop, calls=%fused_computation.2 | loop fusion | flops 6290432 | bytes 4198400 | tf_op jit(solution)/shard_map/reduce_sum | solution.py:78
  10.0 2.4 %fusion.38 = bf16[64,1,1024]{2,0,1:T(8,128)(2,1)S(1)} fusion(bf16[2048,64]{0,1:T(8,128)(2,1)} %param.6, bf16[1024,2048]{1,0:T(8,128)(2,1)S(1)} %copy-done.1, f32[2048]{0:T(1024)S(1)} %copy-done.2, f32[1024]{0:T(1024)S(1)} %add_rsqrt_fusion), kind=kOutput, calls=%fused_computation.44 | convolution fusion | flops 276889600 | bytes 4599808 | tf_op jit(solution)/shard_map/dot_general | solution.py:80
  12.4 0.5 broadcast.165
  13.0 0.7 reduce.1
  13.6 0.7 reshape.90
  14.3 13.9 %all-to-all-start = ((bf16[32,2,1024]{2,1,0:T(2,128)(2,1)}), bf16[32,2,1024]{2,1,0:T(2,128)(2,1)S(1)}, u32[]{:S(2)}, u32[]{:S(2)}) async-start(bf16[32,2,1024]{2,1,0:T(2,128)(2,1)} %reshape.90), calls=%async_computation | async-start | bytes 262144 | tf_op jit(solution)/shard_map/all_to_all | solution.py:92
  28.2 0.5 fusion.78
  28.8 8.6 %all-to-all-done = bf16[32,2,1024]{2,1,0:T(2,128)(2,1)S(1)} async-done(((bf16[32,2,1024]{2,1,0:T(2,128)(2,1)}), bf16[32,2,1024]{2,1,0:T(2,128)(2,1)S(1)}, u32[]{:S(2)}, u32[]{:S(2)}) %all-to-all-start) | async-done | bytes 131104 | tf_op jit(solution)/shard_map/all_to_all | solution.py:92
  37.5 0.7 reduce
  38.9 8.7 %fusion.21 = f32[128,512]{1,0:T(8,128)S(1)} fusion(f32[64,1024]{1,0:T(8,128)S(1)} %bitcast.98, f32[64,1024]{1,0:T(8,128)S(1)} %bitcast.94), kind=kOutput, calls=%fused_computation.28 | convolution fusion | flops 410124288 | bytes 786432 | tf_op jit(solution)/shard_map/dot_general | solution.py:59
  47.6 8.6 %fusion.17 = f32[128,512]{1,0:T(8,128)S(1)} fusion(s32[512]{0:T(512)S(1)} %iota_add_fusion, f32[64,1024]{1,0:T(8,128)S(1)} %bitcast.99, f32[64,1024]{1,0:T(8,128)S(1)} %bitcast.95), kind=kOutput, calls=%fused_computation.24 | convolution fusion | flops 410124288 | bytes 788480 | tf_op jit(solution)/shard_map/dot_general | solution.py:58
  56.2 8.9 %fusion.15 = f32[128,512]{1,0:T(8,128)S(1)} fusion(s32[512]{0:T(512)S(1)} %iota_add_fusion, f32[64,1024]{1,0:T(8,128)S(1)} %bitcast.100, f32[64,1024]{1,0:T(8,128)S(1)} %bitcast.96), kind=kOutput, calls=%fused_computation.22 | convolution fusion | flops 410124288 | bytes 788480 | tf_op jit(solution)/shard_map/dot_general | solution.py:59
  65.1 8.6 %fusion.23 = f32[128,512]{1,0:T(8,128)S(1)} fusion(f32[64,1024]{1,0:T(8,128)S(1)} %bitcast.101, f32[64,1024]{1,0:T(8,128)S(1)} %bitcast.97), kind=kOutput, calls=%fused_computation.30 | convolution fusion | flops 410124288 | bytes 786432 | tf_op jit(solution)/shard_map/dot_general | solution.py:58
  73.9 0.4 convert_element_type.108
  74.2 0.7 copy.35
  74.9 0.4 convert_element_type.107
  75.3 0.7 copy.34
  76.2 0.4 reshape.92
  76.6 13.7 %all_to_all.66 = bf16[32,2,2048]{2,1,0:T(2,128)(2,1)S(1)} all-to-all(bf16[32,2,2048]{2,1,0:T(2,128)(2,1)S(1)} %reshape.92), channel_id=1, replica_groups=mesh['row'=32,'col'=16] {'row'}, dimensions={0} | all-to-all | bytes 524288 | tf_op jit(solution)/shard_map/all_to_all | solution.py:19
  90.9 0.6 copy.41
  91.5 0.9 reshape.96
  92.4 10.9 %all-to-all-start.3 = ((bf16[16,2,2048]{2,1,0:T(2,128)(2,1)}), bf16[16,2,2048]{2,1,0:T(2,128)(2,1)S(1)}, u32[]{:S(2)}, u32[]{:S(2)}) async-start(bf16[16,2,2048]{2,1,0:T(2,128)(2,1)} %reshape.96), calls=%async_computation.3 | async-start | bytes 262144 | tf_op jit(solution)/shard_map/all_to_all | solution.py:141
  103.3 0.6 copy.37
  103.9 0.9 reshape.94
  104.8 7.4 %all-to-all-done.3 = bf16[16,2,2048]{2,1,0:T(2,128)(2,1)S(1)} async-done(((bf16[16,2,2048]{2,1,0:T(2,128)(2,1)}), bf16[16,2,2048]{2,1,0:T(2,128)(2,1)S(1)}, u32[]{:S(2)}, u32[]{:S(2)}) %all-to-all-start.3) | async-done | bytes 131104 | tf_op jit(solution)/shard_map/all_to_all | solution.py:141
  112.2 3.4 %all-to-all-start.2 = ((bf16[16,2,2048]{2,1,0:T(2,128)(2,1)}), bf16[16,2,2048]{2,1,0:T(2,128)(2,1)S(1)}, u32[]{:S(2)}, u32[]{:S(2)}) async-start(bf16[16,2,2048]{2,1,0:T(2,128)(2,1)} %reshape.94), calls=%async_computation.2 | async-start | bytes 262144 | tf_op jit(solution)/shard_map/all_to_all | solution.py:134
  116.3 8.2 %all-to-all-done.2 = bf16[16,2,2048]{2,1,0:T(2,128)(2,1)S(1)} async-done(((bf16[16,2,2048]{2,1,0:T(2,128)(2,1)}), bf16[16,2,2048]{2,1,0:T(2,128)(2,1)S(1)}, u32[]{:S(2)}, u32[]{:S(2)}) %all-to-all-start.2) | async-done | bytes 131104 | tf_op jit(solution)/shard_map/all_to_all | solution.py:134
  125.2 1.2 fusion.49
  126.4 1.2 fusion.37
  127.7 0.7 convert_element_type.118
  128.5 32.2 %all-gather.2.cloned.1.call-done = bf16[1024,1,1024]{0,2,1:T(8,128)(2,1)} async-done(((bf16[1024,1,64]{0,2,1:T(8,128)(2,1)}), bf16[1024,1,1024]{0,2,1:T(8,128)(2,1)}) %all-gather.2.cloned.1.call-update) | async-done | bytes 2097168 | tf_op jit(solution)/shard_map/all_gather | solution.py:160
  160.7 3.0 %fusion.29 = bf16[1024,128]{1,0:T(8,128)(2,1)} fusion(bf16[1024,128]{1,0:T(8,128)(2,1)S(1)} %copy-done, bf16[1024,1,1024]{0,2,1:T(8,128)(2,1)} %all-gather.2.cloned.1.call-done), kind=kOutput, calls=%fused_computation.36 | convolution fusion | flops 268566528 | bytes 2621440 | tf_op jit(solution)/shard_map/dot_general | solution.py:162
  (32 shorter events, 3.4 us)
Async XLA Ops:
  6.5 154.2 %copy-start = (bf16[1024,128]{1,0:T(8,128)(2,1)S(1)}, bf16[1024,128]{1,0:T(8,128)(2,1)}, u32[]{:S(2)}) copy-start(bf16[1024,128]{1,0:T(8,128)(2,1)} %param.7) | copy-start | bytes 786436
  6.5 3.5 %copy-start.1 = (bf16[1024,2048]{1,0:T(8,128)(2,1)S(1)}, bf16[1024,2048]{1,0:T(8,128)(2,1)}, u32[]{:S(2)}) copy-start(bf16[1024,2048]{1,0:T(8,128)(2,1)} %param.4) | copy-start | bytes 12582916
  6.5 3.5 %copy-start.2 = (f32[2048]{0:T(1024)S(1)}, f32[2048]{0:T(1024)}, u32[]{:S(2)}) copy-start(f32[2048]{0:T(1024)} %param.5) | copy-start | bytes 24580
  14.3 23.1 %all-to-all-start = ((bf16[32,2,1024]{2,1,0:T(2,128)(2,1)}), bf16[32,2,1024]{2,1,0:T(2,128)(2,1)S(1)}, u32[]{:S(2)}, u32[]{:S(2)}) async-start(bf16[32,2,1024]{2,1,0:T(2,128)(2,1)} %reshape.90), calls=%async_computation | async-start | bytes 262144 | tf_op jit(solution)/shard_map/all_to_all | solution.py:92
  92.4 19.8 %all-to-all-start.3 = ((bf16[16,2,2048]{2,1,0:T(2,128)(2,1)}), bf16[16,2,2048]{2,1,0:T(2,128)(2,1)S(1)}, u32[]{:S(2)}, u32[]{:S(2)}) async-start(bf16[16,2,2048]{2,1,0:T(2,128)(2,1)} %reshape.96), calls=%async_computation.3 | async-start | bytes 262144 | tf_op jit(solution)/shard_map/all_to_all | solution.py:141
  112.2 12.3 %all-to-all-start.2 = ((bf16[16,2,2048]{2,1,0:T(2,128)(2,1)}), bf16[16,2,2048]{2,1,0:T(2,128)(2,1)S(1)}, u32[]{:S(2)}, u32[]{:S(2)}) async-start(bf16[16,2,2048]{2,1,0:T(2,128)(2,1)} %reshape.94), calls=%async_computation.2 | async-start | bytes 262144 | tf_op jit(solution)/shard_map/all_to_all | solution.py:134
  115.6 45.1 %all-gather.2.cloned.1.call-start = ((), (), s32[]{:S(2)}) async-start(), calls=%async_computation.4 | async-start | bytes 2228224 | tf_op jit(solution)/shard_map/all_gather | solution.py:160
Sparse Core Ops, SparseCore 0:
  128.6 32.0 all-gather.1
where the time goes:
time: 171 us
  waiting for transfers between devices  56.5 us (33%)
  matrix products  43.2 us (25%)
  starting transfers between devices  28.2 us (16%)
  blocking collectives  13.7 us (8%)
  between operations  13.7 us (8%)
  local copies, waits for them, and re-layouts  9.71 us (6%)
  other arithmetic  5.56 us (3%)
    all_gather x1, waiting for transfers between devices, local(): portion = lax.all_gather(result, 'col', axis=2, tiled=True)  32.2 us
    dot_general x2, matrix products, second_section(): with_sin = jnp.dot(stacked, sine, precision=lax.Precision.HIGH)  17.6 us
    dot_general x2, matrix products, second_section(): with_cos = jnp.dot(stacked, cosine, precision=lax.Precision.HIGH)  17.2 us
    all_to_all x1, starting transfers between devices, local(): lax.all_to_all(projected.reshape(channels, 1, length_dev), 'row', split_a...  13.9 us
    all_to_all x1, blocking collectives, in_one_piece(): lax.all_to_all(both, axis, split_axis=split_dim, concat_axis=concat_dim,...  13.7 us
    all_to_all x1, starting transfers between devices, local(): lax.all_to_all(as_sent(spec_imag.reshape(channels, col_count, quarter)),...  10.9 us
    all_to_all x1, waiting for transfers between devices, local(): lax.all_to_all(projected.reshape(channels, 1, length_dev), 'row', split_a...  8.62 us
    all_to_all x1, waiting for transfers between devices, local(): lax.all_to_all(as_sent(spec_real.reshape(channels, col_count, quarter)),...  8.24 us
  transfers between devices with their start and end apart: 4, of which 4 were waited for; matrix products, arithmetic and copies ran while one was open for 2% of the time, Pallas kernels for 0%

commit v1 on v0

--- a/solution.py
+++ b/solution.py
@@ -157,7 +157,10 @@
         "hz,azo->aho", group_sine_table, imaginary_by_group, precision=lax.Precision.HIGH
     )
     result = merged_spectrum.reshape(width_all, 1, item_count).astype(jnp.bfloat16)
-    portion = lax.all_gather(result, "col", axis=2, tiled=True)
+    current_arr = lax.axis_size("col")
+    before = jnp.stack([result] * current_arr, axis=0)
+    found_now = lax.all_to_all(before, "col", 0, 0)
+    portion = jnp.concatenate(found_now, axis=2)
     flat = portion.reshape(portion.shape[0], portion.shape[2])
     output = lax.dot_general(
         flat, w_out, (((0,), (0,)), ((), ())), preferred_element_type=jnp.float32

time: 171 us -> 176 us (1.029)
  blocking collectives: 13.7 us -> 67 us
  waiting for transfers between devices: 56.5 us -> 24.3 us
  between operations: 13.7 us -> 0.29 us
    all_to_all x0 -> x1, blocking collectives: none -> 53.3 us  [local(): found_now = lax.all_to_all(before, 'col', 0, 0)]
    all_gather x1 -> x0, waiting for transfers between devices: 32.2 us -> none  [local(): portion = lax.all_gather(result, 'col', axis=2, tiled=True)]
  transfers between devices with their start and end apart: 4 -> 3, of which waited for: 4 -> 3; matrix products, arithmetic and copies ran while one was open for 2% -> 2% of each run, Pallas kernels for 0% -> 0%
where the time goes in v1:
time: 176 us
  blocking collectives  67 us (38%)
  matrix products  41.6 us (24%)
  starting transfers between devices  28.2 us (16%)
  waiting for transfers between devices  24.3 us (14%)
  local copies, waits for them, and re-layouts  9.13 us (5%)
  other arithmetic  5.56 us (3%)
    all_to_all x1, blocking collectives, local(): found_now = lax.all_to_all(before, 'col', 0, 0)  53.3 us
    dot_general x2, matrix products, second_section(): with_sin = jnp.dot(stacked, sine, precision=lax.Precision.HIGH)  17.6 us
    dot_general x2, matrix products, second_section(): with_cos = jnp.dot(stacked, cosine, precision=lax.Precision.HIGH)  17.2 us
    all_to_all x1, starting transfers between devices, local(): lax.all_to_all(projected.reshape(channels, 1, length_dev), 'row', split_a...  13.9 us
    all_to_all x1, blocking collectives, in_one_piece(): lax.all_to_all(both, axis, split_axis=split_dim, concat_axis=concat_dim,...  13.7 us
    all_to_all x1, starting transfers between devices, local(): lax.all_to_all(as_sent(spec_imag.reshape(channels, col_count, quarter)),...  10.9 us
    all_to_all x1, waiting for transfers between devices, local(): lax.all_to_all(projected.reshape(channels, 1, length_dev), 'row', split_a...  8.62 us
    all_to_all x1, waiting for transfers between devices, local(): lax.all_to_all(as_sent(spec_real.reshape(channels, col_count, quarter)),...  8.29 us
  transfers between devices with their start and end apart: 3, of which 3 were waited for; matrix products, arithmetic and copies ran while one was open for 2% of the time, Pallas kernels for 0%

profile of v1, /device:TPU:1, one launch (start us, length us, event | category | flops | bytes accessed | tf_op | source)
XLA Modules:
  0.0 176.0 jit_solution(3199771472500739213)
XLA Ops:
  0.0 3.2 %fusion = f32[1024]{0:T(1024)S(1)} fusion(bf16[1024,2048]{1,0:T(8,128)(2,1)} %param.4), kind=kLoop, calls=%fused_computation.2 | loop fusion | flops 6290432 | bytes 4198400 | tf_op jit(solution)/shard_map/reduce_sum | solution.py:78
  3.5 2.4 %fusion.33 = bf16[64,1,1024]{2,0,1:T(8,128)(2,1)S(1)} fusion(bf16[2048,64]{0,1:T(8,128)(2,1)} %param.6, bf16[1024,2048]{1,0:T(8,128)(2,1)S(1)} %copy-done.1, f32[2048]{0:T(1024)S(1)} %copy-done.2, f32[1024]{0:T(1024)S(1)} %add_rsqrt_fusion), kind=kOutput, calls=%fused_computation.42 | convolution fusion | flops 276889600 | bytes 4599808 | tf_op jit(solution)/shard_map/dot_general | solution.py:80
  5.9 0.5 broadcast.167
  6.4 0.7 reduce.1
  7.1 0.7 reshape.89
  7.8 13.9 %all-to-all-start = ((bf16[32,2,1024]{2,1,0:T(2,128)(2,1)}), bf16[32,2,1024]{2,1,0:T(2,128)(2,1)S(1)}, u32[]{:S(2)}, u32[]{:S(2)}) async-start(bf16[32,2,1024]{2,1,0:T(2,128)(2,1)} %reshape.89), calls=%async_computation | async-start | bytes 262144 | tf_op jit(solution)/shard_map/all_to_all | solution.py:92
  21.7 0.5 fusion.73
  22.2 8.6 %all-to-all-done = bf16[32,2,1024]{2,1,0:T(2,128)(2,1)S(1)} async-done(((bf16[32,2,1024]{2,1,0:T(2,128)(2,1)}), bf16[32,2,1024]{2,1,0:T(2,128)(2,1)S(1)}, u32[]{:S(2)}, u32[]{:S(2)}) %all-to-all-start) | async-done | bytes 131104 | tf_op jit(solution)/shard_map/all_to_all | solution.py:92
  31.0 0.7 reduce
  32.4 8.7 %fusion.19 = f32[128,512]{1,0:T(8,128)S(1)} fusion(f32[64,1024]{1,0:T(8,128)S(1)} %bitcast.100, f32[64,1024]{1,0:T(8,128)S(1)} %bitcast.96), kind=kOutput, calls=%fused_computation.26 | convolution fusion | flops 410124288 | bytes 786432 | tf_op jit(solution)/shard_map/dot_general | solution.py:59
  41.1 8.6 %fusion.15 = f32[128,512]{1,0:T(8,128)S(1)} fusion(s32[512]{0:T(512)S(1)} %iota_add_fusion, f32[64,1024]{1,0:T(8,128)S(1)} %bitcast.101, f32[64,1024]{1,0:T(8,128)S(1)} %bitcast.97), kind=kOutput, calls=%fused_computation.22 | convolution fusion | flops 410124288 | bytes 788480 | tf_op jit(solution)/shard_map/dot_general | solution.py:58
  49.7 8.9 %fusion.13 = f32[128,512]{1,0:T(8,128)S(1)} fusion(s32[512]{0:T(512)S(1)} %iota_add_fusion, f32[64,1024]{1,0:T(8,128)S(1)} %bitcast.102, f32[64,1024]{1,0:T(8,128)S(1)} %bitcast.98), kind=kOutput, calls=%fused_computation.20 | convolution fusion | flops 410124288 | bytes 788480 | tf_op jit(solution)/shard_map/dot_general | solution.py:59
  58.6 8.6 %fusion.21 = f32[128,512]{1,0:T(8,128)S(1)} fusion(f32[64,1024]{1,0:T(8,128)S(1)} %bitcast.103, f32[64,1024]{1,0:T(8,128)S(1)} %bitcast.99), kind=kOutput, calls=%fused_computation.28 | convolution fusion | flops 410124288 | bytes 786432 | tf_op jit(solution)/shard_map/dot_general | solution.py:58
  67.3 0.4 convert_element_type.107
  67.7 0.7 copy.34
  68.4 0.4 convert_element_type.106
  68.7 0.7 copy.33
  69.7 0.4 reshape.91
  70.1 13.7 %all_to_all.71 = bf16[32,2,2048]{2,1,0:T(2,128)(2,1)S(1)} all-to-all(bf16[32,2,2048]{2,1,0:T(2,128)(2,1)S(1)} %reshape.91), channel_id=1, replica_groups=mesh['row'=32,'col'=16] {'row'}, dimensions={0} | all-to-all | bytes 524288 | tf_op jit(solution)/shard_map/all_to_all | solution.py:19
  83.8 0.4 reshape.92
  84.4 0.6 copy.40
  85.0 0.9 reshape.95
  85.9 10.9 %all-to-all-start.3 = ((bf16[16,2,2048]{2,1,0:T(2,128)(2,1)}), bf16[16,2,2048]{2,1,0:T(2,128)(2,1)S(1)}, u32[]{:S(2)}, u32[]{:S(2)}) async-start(bf16[16,2,2048]{2,1,0:T(2,128)(2,1)} %reshape.95), calls=%async_computation.3 | async-start | bytes 262144 | tf_op jit(solution)/shard_map/all_to_all | solution.py:141
  96.8 0.6 copy.36
  97.4 0.9 reshape.93
  98.3 7.4 %all-to-all-done.3 = bf16[16,2,2048]{2,1,0:T(2,128)(2,1)S(1)} async-done(((bf16[16,2,2048]{2,1,0:T(2,128)(2,1)}), bf16[16,2,2048]{2,1,0:T(2,128)(2,1)S(1)}, u32[]{:S(2)}, u32[]{:S(2)}) %all-to-all-start.3) | async-done | bytes 131104 | tf_op jit(solution)/shard_map/all_to_all | solution.py:141
  105.6 3.4 %all-to-all-start.2 = ((bf16[16,2,2048]{2,1,0:T(2,128)(2,1)}), bf16[16,2,2048]{2,1,0:T(2,128)(2,1)S(1)}, u32[]{:S(2)}, u32[]{:S(2)}) async-start(bf16[16,2,2048]{2,1,0:T(2,128)(2,1)} %reshape.93), calls=%async_computation.2 | async-start | bytes 262144 | tf_op jit(solution)/shard_map/all_to_all | solution.py:134
  109.7 8.3 %all-to-all-done.2 = bf16[16,2,2048]{2,1,0:T(2,128)(2,1)S(1)} async-done(((bf16[16,2,2048]{2,1,0:T(2,128)(2,1)}), bf16[16,2,2048]{2,1,0:T(2,128)(2,1)S(1)}, u32[]{:S(2)}, u32[]{:S(2)}) %all-to-all-start.2) | async-done | bytes 131104 | tf_op jit(solution)/shard_map/all_to_all | solution.py:134
  118.6 1.2 fusion.44
  119.8 1.2 fusion.32
  121.3 53.3 %all_to_all.72 = bf16[16,1024,1,64]{1,3,2,0:T(8,128)(2,1)S(1)} all-to-all(bf16[16,1024,1,64]{1,3,2,0:T(8,128)(2,1)S(1)} %stack.2), channel_id=1, replica_groups=mesh['row'=32,'col'=16] {'col'}, dimensions={0} | all-to-all | bytes 4194304 | tf_op jit(solution)/shard_map/all_to_all | solution.py:162
  174.6 1.4 convolution_convert_fusion
  (30 shorter events, 3.2 us)
Async XLA Ops:
  0.0 174.6 %copy-start = (bf16[1024,128]{1,0:T(8,128)(2,1)S(1)}, bf16[1024,128]{1,0:T(8,128)(2,1)}, u32[]{:S(2)}) copy-start(bf16[1024,128]{1,0:T(8,128)(2,1)} %param.7) | copy-start | bytes 786436
  0.0 3.5 %copy-start.1 = (bf16[1024,2048]{1,0:T(8,128)(2,1)S(1)}, bf16[1024,2048]{1,0:T(8,128)(2,1)}, u32[]{:S(2)}) copy-start(bf16[1024,2048]{1,0:T(8,128)(2,1)} %param.4) | copy-start | bytes 12582916
  0.0 3.5 %copy-start.2 = (f32[2048]{0:T(1024)S(1)}, f32[2048]{0:T(1024)}, u32[]{:S(2)}) copy-start(f32[2048]{0:T(1024)} %param.5) | copy-start | bytes 24580
  7.8 23.1 %all-to-all-start = ((bf16[32,2,1024]{2,1,0:T(2,128)(2,1)}), bf16[32,2,1024]{2,1,0:T(2,128)(2,1)S(1)}, u32[]{:S(2)}, u32[]{:S(2)}) async-start(bf16[32,2,1024]{2,1,0:T(2,128)(2,1)} %reshape.89), calls=%async_computation | async-start | bytes 262144 | tf_op jit(solution)/shard_map/all_to_all | solution.py:92
  85.9 19.8 %all-to-all-start.3 = ((bf16[16,2,2048]{2,1,0:T(2,128)(2,1)}), bf16[16,2,2048]{2,1,0:T(2,128)(2,1)S(1)}, u32[]{:S(2)}, u32[]{:S(2)}) async-start(bf16[16,2,2048]{2,1,0:T(2,128)(2,1)} %reshape.95), calls=%async_computation.3 | async-start | bytes 262144 | tf_op jit(solution)/shard_map/all_to_all | solution.py:141
  105.6 12.3 %all-to-all-start.2 = ((bf16[16,2,2048]{2,1,0:T(2,128)(2,1)}), bf16[16,2,2048]{2,1,0:T(2,128)(2,1)S(1)}, u32[]{:S(2)}, u32[]{:S(2)}) async-start(bf16[16,2,2048]{2,1,0:T(2,128)(2,1)} %reshape.93), calls=%async_computation.2 | async-start | bytes 262144 | tf_op jit(solution)/shard_map/all_to_all | solution.py:134
